TPU v7x, 512 devices: a whole 4x8x8 slice. The times are simulated.
512 devices in a mesh: dp: 4 (over x), kv: 64 (over z, y), tp: 2 (over core).
Axes of the slice: x: 4, y: 8, z: 8, core: 2. Of those that a mesh axis runs over, the one named last changes fastest.
Arguments:
- tokens: bfloat16 [512, 4, 4096], P('dp', None, 'kv'), may hold values from -260 to 260
- norm_gain: bfloat16 [4096], replicated, may hold values from 0.099609375 to 1.8984375
- query_weight: bfloat16 [4096, 2048], P(None, ('tp', 'kv')), may hold values from -0.09375 to 0.09375
- key_weight: bfloat16 [4096, 2048], P(None, ('tp', 'kv')), may hold values from -0.09375 to 0.09375
- value_weight: bfloat16 [4096, 4096], P(None, ('tp', 'kv')), may hold values from -0.09375 to 0.09375
- gate_weight: bfloat16 [4096, 4096], P(None, ('tp', 'kv')), may hold values from -0.09375 to 0.09375
- out_weight: bfloat16 [4096, 4096], P('tp', 'kv'), may hold values from -0.09375 to 0.09375
- decay_rate: float32 [16], P('tp'), may hold values from 0.02 to 1
- prior_state: float32 [512, 16, 128, 256], P(('dp', 'kv'), 'tp'), may hold values from -0.6 to 0.6
- last_keys: bfloat16 [512, 4, 16, 128], P(('dp', 'kv'), None, 'tp'), may hold values from -0.5390625 to 0.5390625
- last_values: bfloat16 [512, 4, 16, 256], P(('dp', 'kv'), None, 'tp'), may hold values from -6 to 6
- accepted: int32 [512], P(('dp', 'kv')), may hold values from 0 to 4
- lengths: int32 [512], P(('dp', 'kv')), may hold values from 16 to 99999
Outputs:
- retained: bfloat16 [512, 4, 4096], P('dp', None, ('kv', 'tp'))
- new_state: float32 [512, 16, 128, 256], P(('dp', 'kv'), 'tp')
- new_keys: bfloat16 [512, 4, 16, 128], P(('dp', 'kv'), None, 'tp')
- new_values: bfloat16 [512, 4, 16, 256], P(('dp', 'kv'), None, 'tp')
Inputs may be any that keep to these rules, and one draw needn't show every extreme that they name: `accepted`: how many of the last step's 4 proposals were taken.
All inputs are finite; a program needn't handle non-finite values.
Results may differ from a plain program's by a relative error of at most 0.012.
Values may be sent and summed in bfloat16 or wider, within the bound.
No kernel may reach another device: no remote copies, remote signals or barrier semaphores. Data moves between devices by JAX's collectives and lax.ppermute only.
A program may use at most 64 MiB of HBM per device.

v0:
```python
import jax
import jax.numpy as jnp
from jax import lax
from jax.sharding import Mesh
from jax.sharding import PartitionSpec as P

KV = ("kv_0", "kv_1")
TP_KV = ("tp", "kv_0", "kv_1")
DP_KV = ("dp", "kv_0", "kv_1")
KV_TP = ("kv_0", "kv_1", "tp")
epsilon = 1e-06


def over_axes(value, axes):
    for axis in axes:
        value = lax.psum(value, axis)
    return value


def swapped(value, axis, bit):
    return lax.ppermute(value, axis, [(i, i ^ 1 << bit) for i in range(lax.axis_size(axis))])


def laid_out(blocks, dim):
    lengths = list(blocks.shape[1:])
    lengths[dim] *= blocks.shape[0]
    return jnp.moveaxis(blocks, 0, dim).reshape(lengths)


def stacked_from(value, axes, turns):
    blocks = value[None]
    for k in turns:
        blocks = lax.all_gather(blocks, axes[k], axis=0, tiled=True)
    carried = [lax.axis_size(axes[k]) for k in reversed(turns)]
    blocks = blocks.reshape(*carried, *value.shape)
    turned = sorted(range(len(turns)), key=lambda place: turns[len(turns) - 1 - place])
    return blocks.transpose(*turned, *range(len(turns), blocks.ndim)).reshape(-1, *value.shape)


def gathered_by_axis(value, axes, turns, dim):
    return laid_out(stacked_from(value, axes, turns), dim)


def in_blocks(value, dim, length):
    before, after = (value.shape[:dim], value.shape[dim + 1 :])
    return jnp.moveaxis(value.reshape(*before, length, -1, *after), dim, 0)


def summed_on_arrival(value, axis, dim):
    length = lax.axis_size(axis)
    blocks = lax.all_to_all(in_blocks(value, dim, length), axis, 0, 0, tiled=True)
    return jnp.sum(blocks.astype(jnp.float32), axis=0)


def rotate(field_in, positions):
    half_size = field_in.shape[-1] // 2
    frequency = jnp.power(10000.0, -jnp.arange(half_size, dtype=jnp.float32) / half_size)
    angles = positions.astype(jnp.float32)[:, :, None, None] * frequency
    cosine, sine_part = (jnp.cos(angles), jnp.sin(angles))
    floats = field_in.astype(jnp.float32)
    first_half, second = (floats[..., :half_size], floats[..., half_size:])
    return jnp.concatenate(
        [first_half * cosine - second * sine_part, first_half * sine_part + second * cosine],
        axis=-1,
    )


def retain(
    query_rot, key_rot, value_rows, prior_state, last_keys, last_values, accepted, log_decay
):
    highest = lax.Precision.HIGHEST
    proposals = query_rot.shape[1]
    step_ids = jnp.arange(proposals, dtype=jnp.int32)
    taken_mask = step_ids[None, :] < accepted[:, None]
    power_exp = jnp.maximum(accepted[:, None] - 1 - step_ids[None, :], 0).astype(jnp.float32)
    weight = jnp.where(
        taken_mask[:, :, None], jnp.exp(log_decay[None, None, :] * power_exp[:, :, None]), 0.0
    )
    carried = jnp.exp(log_decay[None, :] * accepted[:, None].astype(jnp.float32))
    weighted_keys = last_keys.astype(jnp.float32) * weight[..., None]
    taken_state = carried[:, :, None, None] * prior_state + jnp.einsum(
        "sphd,sphe->shde", weighted_keys, last_values.astype(jnp.float32), precision=highest
    )
    scores = jnp.einsum(
        "sthd,smhd->shtm",
        query_rot.astype(jnp.float32),
        key_rot.astype(jnp.float32),
        precision=highest,
    )
    offset = (step_ids[:, None] - step_ids[None, :]).astype(jnp.float32)
    decay_grid = jnp.where(
        offset[None] >= 0.0, jnp.exp(log_decay[:, None, None] * jnp.maximum(offset, 0.0)[None]), 0.0
    )
    inner_sum = jnp.einsum(
        "shtm,smhe->sthe",
        scores * decay_grid[None],
        value_rows.astype(jnp.float32),
        precision=highest,
    )
    query_decay = jnp.exp(log_decay[None, :] * (step_ids[:, None].astype(jnp.float32) + 1.0))
    cross_sum = jnp.einsum(
        "sthd,shde->sthe",
        query_rot.astype(jnp.float32) * query_decay[None, :, :, None],
        taken_state,
        precision=highest,
    )
    return (inner_sum + cross_sum, taken_state)


def row_scale(tokens, row_block, first_row):
    partial_sq = jnp.sum(jnp.square(tokens.astype(jnp.float32)), axis=-1)
    total_sq = over_axes(partial_sq, KV)
    picked = lax.dynamic_slice_in_dim(total_sq, first_row, row_block.shape[1], 1)
    return lax.rsqrt(picked / row_block.shape[-1] + epsilon)


def shards(
    tokens,
    norm_gain,
    query_weight,
    key_weight,
    value_weight,
    gate_weight,
    out_weight,
    decay_rate,
    prior_state,
    last_keys,
    last_values,
    accepted,
    lengths,
):
    groups = lax.axis_size(KV)
    owned_seqs, proposals, _ = tokens.shape
    local_seqs, heads_here, key_size, value_size = prior_state.shape
    width = norm_gain.shape[0]
    key_cols = query_weight.shape[1]
    value_cols = value_weight.shape[1]
    col_span = 2 * key_cols + 2 * value_cols
    gain_vector = norm_gain.astype(jnp.float32)
    pair_index = lax.axis_index("tp")
    half_props = proposals // 2
    own_half = lax.dynamic_slice_in_dim(tokens, pair_index * half_props, half_props, 1)
    gathered = lax.all_gather(own_half, KV, axis=2, tiled=True)
    row_total = gathered.shape[0] * gathered.shape[1]
    scaled = (
        gathered.astype(jnp.float32)
        * row_scale(tokens, gathered, pair_index * half_props)[..., None]
        * gain_vector
    )
    normed = scaled.astype(jnp.bfloat16).reshape(row_total, width)
    own_weights = jnp.concatenate([query_weight, key_weight, value_weight, gate_weight], axis=1)
    other_weights = swapped(own_weights, "tp", 0)
    both_weights = jnp.where(
        pair_index == 0,
        jnp.concatenate([own_weights, other_weights], axis=1),
        jnp.concatenate([other_weights, own_weights], axis=1),
    )
    columns = jnp.dot(normed, both_weights, preferred_element_type=jnp.float32).astype(jnp.bfloat16)
    columns = columns.reshape(owned_seqs, half_props, 2 * col_span)
    arrived = lax.all_to_all(columns, KV, split_axis=0, concat_axis=2, tiled=True)
    arrived = arrived.reshape(local_seqs, half_props, groups, 2 * col_span)
    lower_part = arrived[..., :col_span]
    upper_part = arrived[..., col_span:]
    kept_part = jnp.where(pair_index == 0, lower_part, upper_part)
    sent_part = jnp.where(pair_index == 0, upper_part, lower_part)
    received = swapped(sent_part, "tp", 0)
    assembled = jnp.where(
        pair_index == 0,
        jnp.concatenate([kept_part, received], axis=1),
        jnp.concatenate([received, kept_part], axis=1),
    )

    def role_rows(first_col, col_count, last_size):
        picked = assembled[..., first_col : first_col + col_count]
        return picked.reshape(local_seqs, proposals, heads_here, last_size)

    query_rows = role_rows(0, key_cols, key_size)
    key_rows = role_rows(key_cols, key_cols, key_size)
    value_rows = role_rows(2 * key_cols, value_cols, value_size)
    gate_rows = role_rows(2 * key_cols + value_cols, value_cols, value_size)
    positions = (lengths + accepted)[:, None] + jnp.arange(proposals, dtype=jnp.int32)[None, :]
    query_rot = rotate(query_rows, positions).astype(jnp.bfloat16)
    key_rot = (rotate(key_rows, positions) * key_size ** (-0.5)).astype(jnp.bfloat16)
    heads_out, taken_state = retain(
        query_rot, key_rot, value_rows, prior_state, last_keys, last_values, accepted, -decay_rate
    )
    head_norm = heads_out * lax.rsqrt(
        jnp.mean(heads_out * heads_out, axis=-1, keepdims=True) + epsilon
    )
    gated = (jax.nn.silu(gate_rows.astype(jnp.float32)) * head_norm).astype(jnp.bfloat16)
    gated = gated.reshape(local_seqs, proposals, heads_here * value_size)
    gathered_piece = gathered_by_axis(gated, KV, (0, 1), 0)
    piece_rows = gathered_piece.shape[0]
    flat_rows = gathered_piece.reshape(piece_rows * proposals, heads_here * value_size)
    product = jnp.dot(flat_rows, out_weight, preferred_element_type=jnp.float32)
    partial_terms = product.reshape(piece_rows, proposals, out_weight.shape[1])
    retained = summed_on_arrival(partial_terms.astype(jnp.bfloat16), "tp", 2).astype(jnp.bfloat16)
    return (retained, taken_state, key_rot, value_rows)


def solution(mesh):
    finer = Mesh(
        mesh.devices.reshape(mesh.shape["dp"], 8, 8, mesh.shape["tp"]), ("dp", "kv_0", "kv_1", "tp")
    )
    return jax.shard_map(
        shards,
        mesh=finer,
        in_specs=(
            P("dp", None, KV),
            P(),
            P(None, TP_KV),
            P(None, TP_KV),
            P(None, TP_KV),
            P(None, TP_KV),
            P("tp", KV),
            P("tp"),
            P(DP_KV, "tp", None, None),
            P(DP_KV, None, "tp", None),
            P(DP_KV, None, "tp", None),
            P(DP_KV),
            P(DP_KV),
        ),
        out_specs=(
            P("dp", None, KV_TP),
            P(DP_KV, "tp", None, None),
            P(DP_KV, None, "tp", None),
            P(DP_KV, None, "tp", None),
        ),
        check_vma=False,
    )
```

profile of v0, /device:TPU:1, one launch (start us, length us, event | category | flops | bytes accessed | tf_op | source)
XLA Modules:
  0.0 229.2 jit_solution(18437961642913602430)
XLA Ops:
  7.3 1.6 constant_dynamic-slice_fusion
  8.9 2.0 pad_maximum_fusion
  11.0 8.7 %collective-permute-start = (bf16[4096,96]{0,1:T(8,128)(2,1)}, bf16[4096,96]{0,1:T(8,128)(2,1)}, u32[]{:S(2)}, u32[]{:S(2)}) collective-permute-start(bf16[4096,96]{0,1:T(8,128)(2,1)} %pad_maximum_fusion), channel_id=1, source_target_pairs={{0,1},{1,0},{2,3},{3,2},{4,5},{5,4},{6,7},{7,6},{8,9},{9,8},{10,11... | collective-permute-start | bytes 2359304 | tf_op jit(solution)/shard_map/ppermute | solution.py:21
  21.0 14.1 %psum.14 = f32[128,4]{0,1:T(4,128)S(1)} all-reduce(f32[128,4]{0,1:T(4,128)S(1)} %multiply_reduce_fusion), channel_id=1, replica_groups=mesh['dp'=4,'kv_0'=8,'kv_1'=8,'tp'=2] {'kv_0'}, use_global_device_ids=true, to_apply=%region_1.0 | all-reduce | flops 512 | bytes 4096 | tf_op jit(solution)/shard_map/psum | solution.py:16
  35.1 15.0 %psum.15 = f32[128,4]{0,1:T(4,128)S(1)} all-reduce(f32[128,4]{0,1:T(4,128)S(1)} %psum.14), channel_id=1, replica_groups=mesh['dp'=4,'kv_0'=8,'kv_1'=8,'tp'=2] {'kv_1'}, use_global_device_ids=true, to_apply=%region_2.0 | all-reduce | flops 512 | bytes 4096 | tf_op jit(solution)/shard_map/psum | solution.py:16
  51.5 2.8 %multiply_add_fusion = f32[2,8,128,256]{3,2,1,0:T(8,128)S(1)} fusion(f32[2,8,128,256]{3,2,1,0:T(8,128)} %param.21, f32[2,8]{1,0:T(2,128)S(1)} %multiply_exponential_fusion.1, bf16[2,4,8,256]{3,2,1,0:T(8,128)(2,1)S(1)} %copy-done.8, f32[2,4,8,128]{3,2,1,0:T(8,128)S(1)} %convert_multiply_fusion), kind=kOutput, calls=%fused_computation.2 | convolution fusion | flops 26214400 | bytes 4259904 | tf_op jit(solution)/shard_map/sphd,sphe->shde/dot_general | solution.py:81
  55.2 2.5 %constant_dynamic-update-slice_fusion.9 = (bf16[4096,192]{0,1:T(8,128)(2,1)}, bf16[4096,192]{0,1:T(8,128)(2,1)}) fusion(bf16[4096,96]{0,1:T(8,128)(2,1)} %collective-permute-done, bf16[4096,192]{0,1:T(8,128)(2,1)} %constant_dynamic-update-slice_fusion.1), kind=kLoop, calls=%fused_computation.49 | loop fusion | bytes 2359296
  60.4 36.0 %all-gather.3.cloned.1.call-done = bf16[128,2,4096]{0,2,1:T(8,128)(2,1)} async-done(((bf16[128,2,64]{0,2,1:T(8,128)(2,1)}), bf16[128,2,4096]{0,2,1:T(8,128)(2,1)}) %all-gather.3.cloned.1.call-update) | async-done | bytes 2097168 | tf_op jit(solution)/shard_map/all_gather | solution.py:143
  96.4 2.9 %multiply_convert_fusion = bf16[128,2,4096]{0,2,1:T(8,128)(2,1)} fusion(bf16[128,2,4096]{0,2,1:T(8,128)(2,1)} %all-gather.3.cloned.1.call-done, f32[4096]{0:T(1024)S(1)} %convert_element_type.96, f32[128,2]{0,1:T(2,128)S(1)} %add_rsqrt_fusion.1), kind=kLoop, calls=%fused_computation | loop fusion | flops 4194304 | bytes 4211712 | tf_op jit(solution)/shard_map/convert_element_type | solution.py:150
  99.3 6.2 %copy.63 = bf16[128,2,4096]{2,1,0:T(2,128)(2,1)} copy(bf16[128,2,4096]{0,2,1:T(8,128)(2,1)} %multiply_convert_fusion) | data formatting | bytes 4194304 | tf_op jit(solution)/shard_map/convert_element_type | solution.py:150
  105.5 4.1 %reshape.228 = bf16[256,4096]{1,0:T(8,128)(2,1)} reshape(bf16[128,2,4096]{2,1,0:T(2,128)(2,1)} %copy.63) | data formatting | bytes 4194304 | tf_op jit(solution)/shard_map/reshape | solution.py:150
  109.7 2.9 %fusion.3 = bf16[256,192]{0,1:T(8,128)(2,1)S(1)} fusion(bf16[256,4096]{1,0:T(8,128)(2,1)} %reshape.228, bf16[4096,192]{0,1:T(8,128)(2,1)} %get-tuple-element.21, bf16[4096,192]{0,1:T(8,128)(2,1)} %constant_dynamic-update-slice_fusion.5, pred[]{:T(512)S(6)} %eq.2), kind=kOutput, calls=%fused_computation.6 | convolution fusion | flops 403488768 | bytes 5341185 | tf_op jit(solution)/shard_map/dot_general | solution.py:158
  113.4 8.5 %all-to-all-start = ((bf16[128,2,192]{2,1,0:T(2,128)(2,1)}), bf16[128,2,192]{2,1,0:T(2,128)(2,1)S(1)}, u32[]{:S(2)}, u32[]{:S(2)}) async-start(bf16[128,2,192]{2,1,0:T(2,128)(2,1)} %reshape.229), calls=%async_computation | async-start | bytes 262144 | tf_op jit(solution)/shard_map/all_to_all | solution.py:160
  122.1 11.4 %all-to-all-done = bf16[128,2,192]{2,1,0:T(2,128)(2,1)S(1)} async-done(((bf16[128,2,192]{2,1,0:T(2,128)(2,1)}), bf16[128,2,192]{2,1,0:T(2,128)(2,1)S(1)}, u32[]{:S(2)}, u32[]{:S(2)}) %all-to-all-start) | async-done | bytes 98336 | tf_op jit(solution)/shard_map/all_to_all | solution.py:160
  133.7 8.2 %collective-permute-start.1 = (bf16[2,2,64,96]{3,2,1,0:T(8,128)(2,1)S(1)}, bf16[2,2,64,96]{3,2,1,0:T(8,128)(2,1)S(1)}, u32[]{:S(2)}, u32[]{:S(2)}) collective-permute-start(bf16[2,2,64,96]{3,2,1,0:T(8,128)(2,1)S(1)} %get-tuple-element.27), channel_id=1, source_target_pairs={{0,1},{1,0},{2,3},{3,2},{4,5},{5,4},{6,7},{7,6},{8,9},{9,8},{10,11... | collective-permute-start | bytes 147464 | tf_op jit(solution)/shard_map/ppermute | solution.py:21
  141.9 0.8 collective-permute-done.1
  144.1 1.2 fusion.15
  145.7 20.6 %all_gather.10 = bf16[8,2,4,2048]{3,2,1,0:T(4,128)(2,1)} all-gather(bf16[1,2,4,2048]{3,2,1,0:T(4,128)(2,1)S(1)} %broadcast_in_dim_reshape.3), channel_id=1, replica_groups=mesh['dp'=4,'kv_0'=8,'kv_1'=8,'tp'=2] {'kv_0'}, dimensions={0}, use_global_device_ids=true | all-gather | bytes 294912 | tf_op jit(solution)/shard_map/all_gather | solution.py:33
  167.0 37.0 %all-gather.5.cloned.1.call-done = bf16[64,2,4,2048]{3,2,1,0:T(4,128)(2,1)} async-done(((bf16[8,2,4,2048]{3,2,1,0:T(4,128)(2,1)}), bf16[64,2,4,2048]{3,2,1,0:T(4,128)(2,1)}) %all-gather.5.cloned.1.call-update) | async-done | bytes 2097168 | tf_op jit(solution)/shard_map/all_gather | solution.py:33
  204.0 2.7 %copy.110 = bf16[64,2,4,2048]{3,0,2,1:T(8,128)(2,1)S(1)} copy(bf16[64,2,4,2048]{3,2,1,0:T(4,128)(2,1)} %all-gather.5.cloned.1.call-done) | data formatting | bytes 4194304 | tf_op jit(solution)/shard_map/all_gather | solution.py:33
  206.7 2.2 copy.76
  208.9 2.2 dot_general.25
  211.1 2.3 %convolution_convert_fusion = bf16[128,4,64]{0,2,1:T(8,128)(2,1)S(1)} fusion(bf16[128,4,2048]{2,0,1:T(8,128)(2,1)} %dot_general.25, bf16[2048,64]{0,1:T(8,128)(2,1)S(1)} %copy-done), kind=kOutput, calls=%fused_computation.7 | convolution fusion | flops 134250496 | bytes 2424832 | tf_op jit(solution)/shard_map/dot_general | solution.py:195
  213.5 8.3 %all_to_all.20 = bf16[2,128,4,32]{1,3,2,0:T(8,128)(2,1)S(1)} all-to-all(bf16[2,128,4,32]{1,3,2,0:T(8,128)(2,1)S(1)} %bitcast.46), channel_id=1, replica_groups=mesh['dp'=4,'kv_0'=8,'kv_1'=8,'tp'=2] {'tp'}, dimensions={0} | all-to-all | bytes 131072 | tf_op jit(solution)/shard_map/all_to_all | solution.py:51
  (81 shorter events, 10.4 us)
Async XLA Ops:
  7.2 204.0 %copy-start = (bf16[2048,64]{0,1:T(8,128)(2,1)S(1)}, bf16[2048,64]{0,1:T(8,128)(2,1)}, u32[]{:S(2)}) copy-start(bf16[2048,64]{0,1:T(8,128)(2,1)} %param.19) | copy-start | bytes 786436
  7.2 12.5 %copy-start.6 = (bf16[128,4,64]{0,2,1:T(8,128)(2,1)S(1)}, bf16[128,4,64]{0,2,1:T(8,128)(2,1)}, u32[]{:S(2)}) copy-start(bf16[128,4,64]{0,2,1:T(8,128)(2,1)} %param.13) | copy-start | bytes 196612
  7.2 12.6 %copy-start.4 = (bf16[4096,16]{0,1:T(8,128)(2,1)S(1)}, bf16[4096,16]{0,1:T(8,128)(2,1)}, u32[]{:S(2)}) copy-start(bf16[4096,16]{0,1:T(8,128)(2,1)} %param.15) | copy-start | bytes 393220
  7.2 42.9 %copy-start.5 = (bf16[4096,16]{0,1:T(8,128)(2,1)S(1)}, bf16[4096,16]{0,1:T(8,128)(2,1)}, u32[]{:S(2)}) copy-start(bf16[4096,16]{0,1:T(8,128)(2,1)} %param.16) | copy-start | bytes 393220
  7.2 43.6 %copy-start.2 = (bf16[4096,32]{0,1:T(8,128)(2,1)S(1)}, bf16[4096,32]{0,1:T(8,128)(2,1)}, u32[]{:S(2)}) copy-start(bf16[4096,32]{0,1:T(8,128)(2,1)} %param.17) | copy-start | bytes 786436
  7.2 13.2 %copy-start.12 = (s32[2]{0:T(128)S(1)}, s32[2]{0:T(128)}, u32[]{:S(2)}) copy-start(s32[2]{0:T(128)} %param.24) | copy-start | bytes 28
  7.2 13.3 %copy-start.11 = (s32[2]{0:T(128)S(1)}, s32[2]{0:T(128)}, u32[]{:S(2)}) copy-start(s32[2]{0:T(128)} %param.25) | copy-start | bytes 28
  7.2 13.3 %copy-start.13 = (f32[8]{0:T(128)S(1)}, f32[8]{0:T(128)}, u32[]{:S(2)}) copy-start(f32[8]{0:T(128)} %param.20) | copy-start | bytes 100
  7.3 13.6 %copy-start.9 = (bf16[2,4,8,128]{3,2,1,0:T(8,128)(2,1)S(1)}, bf16[2,4,8,128]{3,2,1,0:T(8,128)(2,1)}, u32[]{:S(2)}) copy-start(bf16[2,4,8,128]{3,2,1,0:T(8,128)(2,1)} %param.22) | copy-start | bytes 49156
  7.3 13.7 %copy-start.10 = (bf16[4096]{0:T(1024)(128)(2,1)S(1)}, bf16[4096]{0:T(1024)(128)(2,1)}, u32[]{:S(2)}) copy-start(bf16[4096]{0:T(1024)(128)(2,1)} %param.14) | copy-start | bytes 24580
  7.3 44.3 %copy-start.8 = (bf16[2,4,8,256]{3,2,1,0:T(8,128)(2,1)S(1)}, bf16[2,4,8,256]{3,2,1,0:T(8,128)(2,1)}, u32[]{:S(2)}) copy-start(bf16[2,4,8,256]{3,2,1,0:T(8,128)(2,1)} %param.23) | copy-start | bytes 98308
  7.3 89.1 %all-gather.3.cloned.1.call-start = ((), (), s32[]{:S(2)}) async-start(), calls=%async_computation.2 | async-start | bytes 2129920 | tf_op jit(solution)/shard_map/all_gather | solution.py:143
  11.0 44.2 %collective-permute-start = (bf16[4096,96]{0,1:T(8,128)(2,1)}, bf16[4096,96]{0,1:T(8,128)(2,1)}, u32[]{:S(2)}, u32[]{:S(2)}) collective-permute-start(bf16[4096,96]{0,1:T(8,128)(2,1)} %pad_maximum_fusion), channel_id=1, source_target_pairs={{0,1},{1,0},{2,3},{3,2},{4,5},{5,4},{6,7},{7,6},{8,9},{9,8},{10,11... | collective-permute-start | bytes 2359304 | tf_op jit(solution)/shard_map/ppermute | solution.py:21
  51.5 2.8 %copy-start.3 = (bf16[4096,32]{0,1:T(8,128)(2,1)S(1)}, bf16[4096,32]{0,1:T(8,128)(2,1)}, u32[]{:S(2)}) copy-start(bf16[4096,32]{0,1:T(8,128)(2,1)} %param.18) | copy-start | bytes 786436
  54.4 89.7 %copy-start.1 = (f32[2,8,128,256]{3,2,1,0:T(8,128)}, f32[2,8,128,256]{3,2,1,0:T(8,128)S(1)}, u32[]{:S(2)}) copy-start(f32[2,8,128,256]{3,2,1,0:T(8,128)S(1)} %multiply_add_fusion) | copy-start | bytes 6291460
  113.4 20.1 %all-to-all-start = ((bf16[128,2,192]{2,1,0:T(2,128)(2,1)}), bf16[128,2,192]{2,1,0:T(2,128)(2,1)S(1)}, u32[]{:S(2)}, u32[]{:S(2)}) async-start(bf16[128,2,192]{2,1,0:T(2,128)(2,1)} %reshape.229), calls=%async_computation | async-start | bytes 262144 | tf_op jit(solution)/shard_map/all_to_all | solution.py:160
  122.0 82.0 %all-gather.5.cloned.1.call-start = ((), (), s32[]{:S(2)}) async-start(), calls=%async_computation.3 | async-start | bytes 2359296 | tf_op jit(solution)/shard_map/all_gather | solution.py:33
  133.7 9.1 %collective-permute-start.1 = (bf16[2,2,64,96]{3,2,1,0:T(8,128)(2,1)S(1)}, bf16[2,2,64,96]{3,2,1,0:T(8,128)(2,1)S(1)}, u32[]{:S(2)}, u32[]{:S(2)}) collective-permute-start(bf16[2,2,64,96]{3,2,1,0:T(8,128)(2,1)S(1)} %get-tuple-element.27), channel_id=1, source_target_pairs={{0,1},{1,0},{2,3},{3,2},{4,5},{5,4},{6,7},{7,6},{8,9},{9,8},{10,11... | collective-permute-start | bytes 147464 | tf_op jit(solution)/shard_map/ppermute | solution.py:21
  143.4 2.0 copy-start.7
Sparse Core Ops, SparseCore 0:
  11.7 84.6 all-gather.2
  166.5 37.4 all-gather.4
where the time goes:
time: 230 us; the launch traced here: 229 us
  waiting for transfers between devices  85.2 us (37%)
  blocking collectives  58 us (25%)
  local copies, waits for them, and re-layouts  29.3 us (13%)
  starting transfers between devices  25.6 us (11%)
  between operations  14.4 us (6%)
  matrix products  9.71 us (4%)
  other arithmetic  7.02 us (3%)
    all_gather x1, waiting for transfers between devices, stacked_from(): blocks = lax.all_gather(blocks, axes[k], axis=0, tiled=True)  37 us
    all_gather x1, waiting for transfers between devices, shards(): gathered = lax.all_gather(own_half, KV, axis=2, tiled=True)  36 us
    psum x2, blocking collectives, over_axes(): value = lax.psum(value, axis)  29.1 us
    all_gather x1, blocking collectives, stacked_from(): blocks = lax.all_gather(blocks, axes[k], axis=0, tiled=True)  20.6 us
    ppermute x2, starting transfers between devices, swapped(): lax.ppermute(value, axis, [(i, i ^ 1 << bit) for i in range(lax.axis_size...  16.9 us
    all_to_all x1, waiting for transfers between devices, shards(): lax.all_to_all(columns, KV, split_axis=0, concat_axis=2, tiled=True)  11.4 us
    all_to_all x1, starting transfers between devices, shards(): lax.all_to_all(columns, KV, split_axis=0, concat_axis=2, tiled=True)  8.55 us
    all_to_all x1, blocking collectives, summed_on_arrival(): lax.all_to_all(in_blocks(value, dim, length), axis, 0, 0, tiled=True)  8.27 us
  transfers between devices with their start and end apart: 5, of which 4 were waited for; matrix products, arithmetic and copies ran while one was open for 6% of the time, Pallas kernels for 0%

commit v1 on v0

--- a/solution.py
+++ b/solution.py
@@ -30,7 +30,10 @@
 def stacked_from(value, axes, turns):
     blocks = value[None]
     for k in turns:
-        blocks = lax.all_gather(blocks, axes[k], axis=0, tiled=True)
+        load = axes[k]
+        blocks = jnp.concatenate(
+            lax.all_to_all(jnp.stack([blocks] * lax.psum(1, load), axis=0), load, 0, 0), axis=0
+        )
     carried = [lax.axis_size(axes[k]) for k in reversed(turns)]
     blocks = blocks.reshape(*carried, *value.shape)
     turned = sorted(range(len(turns)), key=lambda place: turns[len(turns) - 1 - place])

time: 230 us -> 239 us (1.039)
  waiting for transfers between devices: 85.2 us -> 95.7 us
  blocking collectives: 58 us -> 51.3 us
  starting transfers between devices: 25.6 us -> 29.1 us
  local copies, waits for them, and re-layouts: 29.3 us -> 32.3 us
    all_to_all x0 -> x1, waiting for transfers between devices: none -> 47.5 us  [stacked_from(): lax.all_to_all(jnp.stack([blocks] * lax.psum(1, load), axis=0), load, 0, 0)]
    all_gather x1 -> x0, waiting for transfers between devices: 37 us -> none  [stacked_from(): blocks = lax.all_gather(blocks, axes[k], axis=0, tiled=True)]
    all_gather x1 -> x0, blocking collectives: 20.6 us -> none  [stacked_from(): blocks = lax.all_gather(blocks, axes[k], axis=0, tiled=True)]
    all_to_all x0 -> x1, blocking collectives: none -> 14.7 us  [stacked_from(): lax.all_to_all(jnp.stack([blocks] * lax.psum(1, load), axis=0), load, 0, 0)]
    another operation x1 -> x5, local copies, waits for them, and re-layouts: 0.02 us -> 3.64 us  [stacked_from(): jnp.stack([blocks] * lax.psum(1, load), axis=0)]
    all_to_all x0 -> x1, starting transfers between devices: none -> 3.6 us  [stacked_from(): lax.all_to_all(jnp.stack([blocks] * lax.psum(1, load), axis=0), load, 0, 0)]
    all_gather x1 -> x0, local copies, waits for them, and re-layouts: 2.74 us -> none  [stacked_from(): blocks = lax.all_gather(blocks, axes[k], axis=0, tiled=True)]
where the time goes in v1:
time: 239 us; the launch traced here: 238 us
  waiting for transfers between devices  95.7 us (40%)
  blocking collectives  51.3 us (21%)
  local copies, waits for them, and re-layouts  32.3 us (14%)
  starting transfers between devices  29.1 us (12%)
  between operations  14.4 us (6%)
  matrix products  8.12 us (3%)
  other arithmetic  7.02 us (3%)
    all_to_all x1, waiting for transfers between devices, stacked_from(): lax.all_to_all(jnp.stack([blocks] * lax.psum(1, load), axis=0), load, 0, 0)  47.5 us
    all_gather x1, waiting for transfers between devices, shards(): gathered = lax.all_gather(own_half, KV, axis=2, tiled=True)  36 us
    psum x2, blocking collectives, over_axes(): value = lax.psum(value, axis)  29.1 us
    ppermute x2, starting transfers between devices, swapped(): lax.ppermute(value, axis, [(i, i ^ 1 << bit) for i in range(lax.axis_size...  16.9 us
    all_to_all x1, blocking collectives, stacked_from(): lax.all_to_all(jnp.stack([blocks] * lax.psum(1, load), axis=0), load, 0, 0)  14.7 us
    all_to_all x1, waiting for transfers between devices, shards(): lax.all_to_all(columns, KV, split_axis=0, concat_axis=2, tiled=True)  11.5 us
    all_to_all x1, starting transfers between devices, shards(): lax.all_to_all(columns, KV, split_axis=0, concat_axis=2, tiled=True)  8.55 us
    unnamed x37, local copies, waits for them, and re-layouts  8.08 us
  transfers between devices with their start and end apart: 5, of which 4 were waited for; matrix products, arithmetic and copies ran while one was open for 6% of the time, Pallas kernels for 0%

profile of v1, /device:TPU:1, one launch (start us, length us, event | category | flops | bytes accessed | tf_op | source)
XLA Modules:
  0.0 237.9 jit_solution(5030548087370064615)
XLA Ops:
  7.3 1.6 constant_dynamic-slice_fusion
  8.9 2.0 pad_maximum_fusion
  11.0 8.7 %collective-permute-start = (bf16[4096,96]{0,1:T(8,128)(2,1)}, bf16[4096,96]{0,1:T(8,128)(2,1)}, u32[]{:S(2)}, u32[]{:S(2)}) collective-permute-start(bf16[4096,96]{0,1:T(8,128)(2,1)} %pad_maximum_fusion), channel_id=1, source_target_pairs={{0,1},{1,0},{2,3},{3,2},{4,5},{5,4},{6,7},{7,6},{8,9},{9,8},{10,11... | collective-permute-start | bytes 2359304 | tf_op jit(solution)/shard_map/ppermute | solution.py:21
  21.0 14.1 %psum.14 = f32[128,4]{0,1:T(4,128)S(1)} all-reduce(f32[128,4]{0,1:T(4,128)S(1)} %multiply_reduce_fusion), channel_id=1, replica_groups=mesh['dp'=4,'kv_0'=8,'kv_1'=8,'tp'=2] {'kv_0'}, use_global_device_ids=true, to_apply=%region_1.0 | all-reduce | flops 512 | bytes 4096 | tf_op jit(solution)/shard_map/psum | solution.py:16
  35.1 15.0 %psum.15 = f32[128,4]{0,1:T(4,128)S(1)} all-reduce(f32[128,4]{0,1:T(4,128)S(1)} %psum.14), channel_id=1, replica_groups=mesh['dp'=4,'kv_0'=8,'kv_1'=8,'tp'=2] {'kv_1'}, use_global_device_ids=true, to_apply=%region_2.0 | all-reduce | flops 512 | bytes 4096 | tf_op jit(solution)/shard_map/psum | solution.py:16
  51.5 2.8 %multiply_add_fusion = f32[2,8,128,256]{3,2,1,0:T(8,128)S(1)} fusion(f32[2,8,128,256]{3,2,1,0:T(8,128)} %param.21, f32[2,8]{1,0:T(2,128)S(1)} %multiply_exponential_fusion.1, bf16[2,4,8,256]{3,2,1,0:T(8,128)(2,1)S(1)} %copy-done.8, f32[2,4,8,128]{3,2,1,0:T(8,128)S(1)} %convert_multiply_fusion), kind=kOutput, calls=%fused_computation.1 | convolution fusion | flops 26214400 | bytes 4259904 | tf_op jit(solution)/shard_map/sphd,sphe->shde/dot_general | solution.py:84
  55.2 2.5 %constant_dynamic-update-slice_fusion.9 = (bf16[4096,192]{0,1:T(8,128)(2,1)}, bf16[4096,192]{0,1:T(8,128)(2,1)}) fusion(bf16[4096,96]{0,1:T(8,128)(2,1)} %collective-permute-done, bf16[4096,192]{0,1:T(8,128)(2,1)} %constant_dynamic-update-slice_fusion.1), kind=kLoop, calls=%fused_computation.48 | loop fusion | bytes 2359296
  60.4 36.0 %all-gather.2.cloned.1.call-done = bf16[128,2,4096]{0,2,1:T(8,128)(2,1)} async-done(((bf16[128,2,64]{0,2,1:T(8,128)(2,1)}), bf16[128,2,4096]{0,2,1:T(8,128)(2,1)}) %all-gather.2.cloned.1.call-update) | async-done | bytes 2097168 | tf_op jit(solution)/shard_map/all_gather | solution.py:146
  96.4 2.9 %multiply_convert_fusion = bf16[128,2,4096]{0,2,1:T(8,128)(2,1)} fusion(bf16[128,2,4096]{0,2,1:T(8,128)(2,1)} %all-gather.2.cloned.1.call-done, f32[4096]{0:T(1024)S(1)} %convert_element_type.96, f32[128,2]{0,1:T(2,128)S(1)} %add_rsqrt_fusion.1), kind=kLoop, calls=%fused_computation | loop fusion | flops 4194304 | bytes 4211712 | tf_op jit(solution)/shard_map/convert_element_type | solution.py:153
  99.3 6.2 %copy.49 = bf16[128,2,4096]{2,1,0:T(2,128)(2,1)} copy(bf16[128,2,4096]{0,2,1:T(8,128)(2,1)} %multiply_convert_fusion) | data formatting | bytes 4194304 | tf_op jit(solution)/shard_map/convert_element_type | solution.py:153
  105.5 4.1 %reshape.231 = bf16[256,4096]{1,0:T(8,128)(2,1)} reshape(bf16[128,2,4096]{2,1,0:T(2,128)(2,1)} %copy.49) | data formatting | bytes 4194304 | tf_op jit(solution)/shard_map/reshape | solution.py:153
  109.7 2.9 %fusion.3 = bf16[256,192]{0,1:T(8,128)(2,1)S(1)} fusion(bf16[256,4096]{1,0:T(8,128)(2,1)} %reshape.231, bf16[4096,192]{0,1:T(8,128)(2,1)} %get-tuple-element.17, bf16[4096,192]{0,1:T(8,128)(2,1)} %constant_dynamic-update-slice_fusion.5, pred[]{:T(512)S(6)} %eq.2), kind=kOutput, calls=%fused_computation.5 | convolution fusion | flops 403488768 | bytes 5341185 | tf_op jit(solution)/shard_map/dot_general | solution.py:161
  113.4 8.5 %all-to-all-start = ((bf16[128,2,192]{2,1,0:T(2,128)(2,1)}), bf16[128,2,192]{2,1,0:T(2,128)(2,1)S(1)}, u32[]{:S(2)}, u32[]{:S(2)}) async-start(bf16[128,2,192]{2,1,0:T(2,128)(2,1)} %reshape.232), calls=%async_computation | async-start | bytes 262144 | tf_op jit(solution)/shard_map/all_to_all | solution.py:163
  122.1 11.5 %all-to-all-done = bf16[128,2,192]{2,1,0:T(2,128)(2,1)S(1)} async-done(((bf16[128,2,192]{2,1,0:T(2,128)(2,1)}), bf16[128,2,192]{2,1,0:T(2,128)(2,1)S(1)}, u32[]{:S(2)}, u32[]{:S(2)}) %all-to-all-start) | async-done | bytes 98336 | tf_op jit(solution)/shard_map/all_to_all | solution.py:163
  133.6 8.2 %collective-permute-start.1 = (bf16[2,2,64,96]{3,2,1,0:T(8,128)(2,1)S(1)}, bf16[2,2,64,96]{3,2,1,0:T(8,128)(2,1)S(1)}, u32[]{:S(2)}, u32[]{:S(2)}) collective-permute-start(bf16[2,2,64,96]{3,2,1,0:T(8,128)(2,1)S(1)} %get-tuple-element.23), channel_id=1, source_target_pairs={{0,1},{1,0},{2,3},{3,2},{4,5},{5,4},{6,7},{7,6},{8,9},{9,8},{10,11... | collective-permute-start | bytes 147464 | tf_op jit(solution)/shard_map/ppermute | solution.py:21
  141.9 0.8 collective-permute-done.1
  144.1 1.2 fusion.15
  145.9 14.7 %all_to_all.30 = bf16[8,1,2,4,2048]{4,2,3,1,0:T(2,128)(2,1)S(1)} all-to-all(bf16[8,1,2,4,2048]{4,2,3,1,0:T(2,128)(2,1)S(1)} %stack.6), channel_id=1, replica_groups=mesh['dp'=4,'kv_0'=8,'kv_1'=8,'tp'=2] {'kv_0'}, dimensions={0} | all-to-all | bytes 524288 | tf_op jit(solution)/shard_map/all_to_all | solution.py:35
  160.8 3.2 %stack.7 = bf16[8,8,2,4,2048]{4,2,1,3,0:T(2,128)(2,1)} broadcast(bf16[8,2,4,2048]{3,1,0,2:T(2,128)(2,1)S(1)} %copy.62), dimensions={1,2,3,4} | broadcast | bytes 2359296 | tf_op jit(solution)/shard_map/stack | solution.py:35
  164.1 3.6 %all-to-all-start.2 = ((bf16[8,8,2,4,2048]{4,2,1,3,0:T(2,128)(2,1)}), bf16[8,8,2,4,2048]{4,2,1,3,0:T(2,128)(2,1)S(1)}, u32[]{:S(2)}, u32[]{:S(2)}) async-start(bf16[8,8,2,4,2048]{4,2,1,3,0:T(2,128)(2,1)} %stack.7), calls=%async_computation.2 | async-start | bytes 4194304 | tf_op jit(solution)/shard_map/all_to_all | solution.py:35
  168.3 47.5 %all-to-all-done.2 = bf16[8,8,2,4,2048]{4,2,1,3,0:T(2,128)(2,1)S(1)} async-done(((bf16[8,8,2,4,2048]{4,2,1,3,0:T(2,128)(2,1)}), bf16[8,8,2,4,2048]{4,2,1,3,0:T(2,128)(2,1)S(1)}, u32[]{:S(2)}, u32[]{:S(2)}) %all-to-all-start.2) | async-done | bytes 2097184 | tf_op jit(solution)/shard_map/all_to_all | solution.py:35
  215.7 3.7 %copy.63 = bf16[8,8,2,4,2048]{4,2,1,0,3:T(2,128)(2,1)} copy(bf16[8,8,2,4,2048]{4,2,0,3,1:T(2,128)(2,1)S(1)} %bitcast.39) | data formatting | bytes 4194304 | tf_op jit(solution)/shard_map/transpose | solution.py:40
  219.5 2.7 %dot_general.25 = bf16[128,4,2048]{2,0,1:T(8,128)(2,1)S(1)} reshape(bf16[8,8,2,4,2048]{4,2,1,0,3:T(2,128)(2,1)} %copy.63) | data formatting | bytes 4194304 | tf_op jit(solution)/shard_map/dot_general | solution.py:198
  223.0 7.4 %all_to_all.31 = bf16[2,128,4,32]{1,3,2,0:T(8,128)(2,1)S(1)} all-to-all(bf16[2,128,4,32]{1,3,2,0:T(8,128)(2,1)S(1)} %bitcast.44), channel_id=1, replica_groups=mesh['dp'=4,'kv_0'=8,'kv_1'=8,'tp'=2] {'tp'}, dimensions={0} | all-to-all | bytes 131072 | tf_op jit(solution)/shard_map/all_to_all | solution.py:54
  (83 shorter events, 11.4 us)
Async XLA Ops:
  7.2 215.1 %copy-start = (bf16[2048,64]{0,1:T(8,128)(2,1)S(1)}, bf16[2048,64]{0,1:T(8,128)(2,1)}, u32[]{:S(2)}) copy-start(bf16[2048,64]{0,1:T(8,128)(2,1)} %param.19) | copy-start | bytes 786436
  7.2 12.5 %copy-start.6 = (bf16[128,4,64]{0,2,1:T(8,128)(2,1)S(1)}, bf16[128,4,64]{0,2,1:T(8,128)(2,1)}, u32[]{:S(2)}) copy-start(bf16[128,4,64]{0,2,1:T(8,128)(2,1)} %param.13) | copy-start | bytes 196612
  7.2 12.6 %copy-start.4 = (bf16[4096,16]{0,1:T(8,128)(2,1)S(1)}, bf16[4096,16]{0,1:T(8,128)(2,1)}, u32[]{:S(2)}) copy-start(bf16[4096,16]{0,1:T(8,128)(2,1)} %param.15) | copy-start | bytes 393220
  7.2 42.9 %copy-start.5 = (bf16[4096,16]{0,1:T(8,128)(2,1)S(1)}, bf16[4096,16]{0,1:T(8,128)(2,1)}, u32[]{:S(2)}) copy-start(bf16[4096,16]{0,1:T(8,128)(2,1)} %param.16) | copy-start | bytes 393220
  7.2 43.6 %copy-start.2 = (bf16[4096,32]{0,1:T(8,128)(2,1)S(1)}, bf16[4096,32]{0,1:T(8,128)(2,1)}, u32[]{:S(2)}) copy-start(bf16[4096,32]{0,1:T(8,128)(2,1)} %param.17) | copy-start | bytes 786436
  7.2 13.2 %copy-start.12 = (s32[2]{0:T(128)S(1)}, s32[2]{0:T(128)}, u32[]{:S(2)}) copy-start(s32[2]{0:T(128)} %param.24) | copy-start | bytes 28
  7.2 13.3 %copy-start.11 = (s32[2]{0:T(128)S(1)}, s32[2]{0:T(128)}, u32[]{:S(2)}) copy-start(s32[2]{0:T(128)} %param.25) | copy-start | bytes 28
  7.2 13.3 %copy-start.13 = (f32[8]{0:T(128)S(1)}, f32[8]{0:T(128)}, u32[]{:S(2)}) copy-start(f32[8]{0:T(128)} %param.20) | copy-start | bytes 100
  7.3 13.6 %copy-start.9 = (bf16[2,4,8,128]{3,2,1,0:T(8,128)(2,1)S(1)}, bf16[2,4,8,128]{3,2,1,0:T(8,128)(2,1)}, u32[]{:S(2)}) copy-start(bf16[2,4,8,128]{3,2,1,0:T(8,128)(2,1)} %param.22) | copy-start | bytes 49156
  7.3 13.7 %copy-start.10 = (bf16[4096]{0:T(1024)(128)(2,1)S(1)}, bf16[4096]{0:T(1024)(128)(2,1)}, u32[]{:S(2)}) copy-start(bf16[4096]{0:T(1024)(128)(2,1)} %param.14) | copy-start | bytes 24580
  7.3 44.3 %copy-start.8 = (bf16[2,4,8,256]{3,2,1,0:T(8,128)(2,1)S(1)}, bf16[2,4,8,256]{3,2,1,0:T(8,128)(2,1)}, u32[]{:S(2)}) copy-start(bf16[2,4,8,256]{3,2,1,0:T(8,128)(2,1)} %param.23) | copy-start | bytes 98308
  7.3 89.1 %all-gather.2.cloned.1.call-start = ((), (), s32[]{:S(2)}) async-start(), calls=%async_computation.4 | async-start | bytes 2129920 | tf_op jit(solution)/shard_map/all_gather | solution.py:146
  11.0 44.2 %collective-permute-start = (bf16[4096,96]{0,1:T(8,128)(2,1)}, bf16[4096,96]{0,1:T(8,128)(2,1)}, u32[]{:S(2)}, u32[]{:S(2)}) collective-permute-start(bf16[4096,96]{0,1:T(8,128)(2,1)} %pad_maximum_fusion), channel_id=1, source_target_pairs={{0,1},{1,0},{2,3},{3,2},{4,5},{5,4},{6,7},{7,6},{8,9},{9,8},{10,11... | collective-permute-start | bytes 2359304 | tf_op jit(solution)/shard_map/ppermute | solution.py:21
  51.5 2.8 %copy-start.3 = (bf16[4096,32]{0,1:T(8,128)(2,1)S(1)}, bf16[4096,32]{0,1:T(8,128)(2,1)}, u32[]{:S(2)}) copy-start(bf16[4096,32]{0,1:T(8,128)(2,1)} %param.18) | copy-start | bytes 786436
  54.4 89.7 %copy-start.1 = (f32[2,8,128,256]{3,2,1,0:T(8,128)}, f32[2,8,128,256]{3,2,1,0:T(8,128)S(1)}, u32[]{:S(2)}) copy-start(f32[2,8,128,256]{3,2,1,0:T(8,128)S(1)} %multiply_add_fusion) | copy-start | bytes 6291460
  113.4 20.1 %all-to-all-start = ((bf16[128,2,192]{2,1,0:T(2,128)(2,1)}), bf16[128,2,192]{2,1,0:T(2,128)(2,1)S(1)}, u32[]{:S(2)}, u32[]{:S(2)}) async-start(bf16[128,2,192]{2,1,0:T(2,128)(2,1)} %reshape.232), calls=%async_computation | async-start | bytes 262144 | tf_op jit(solution)/shard_map/all_to_all | solution.py:163
  133.6 9.1 %collective-permute-start.1 = (bf16[2,2,64,96]{3,2,1,0:T(8,128)(2,1)S(1)}, bf16[2,2,64,96]{3,2,1,0:T(8,128)(2,1)S(1)}, u32[]{:S(2)}, u32[]{:S(2)}) collective-permute-start(bf16[2,2,64,96]{3,2,1,0:T(8,128)(2,1)S(1)} %get-tuple-element.23), channel_id=1, source_target_pairs={{0,1},{1,0},{2,3},{3,2},{4,5},{5,4},{6,7},{7,6},{8,9},{9,8},{10,11... | collective-permute-start | bytes 147464 | tf_op jit(solution)/shard_map/ppermute | solution.py:21
  143.4 2.0 copy-start.7
  164.1 51.7 %all-to-all-start.2 = ((bf16[8,8,2,4,2048]{4,2,1,3,0:T(2,128)(2,1)}), bf16[8,8,2,4,2048]{4,2,1,3,0:T(2,128)(2,1)S(1)}, u32[]{:S(2)}, u32[]{:S(2)}) async-start(bf16[8,8,2,4,2048]{4,2,1,3,0:T(2,128)(2,1)} %stack.7), calls=%async_computation.2 | async-start | bytes 4194304 | tf_op jit(solution)/shard_map/all_to_all | solution.py:35
Sparse Core Ops, SparseCore 0:
  11.7 84.6 all-gather.1
